TPU v7x, 128 devices: a whole 4x4x4 slice. The times are simulated.
128 devices in a mesh: sp: 16 (over z, y), dp: 8 (over x, core).
Axes of the slice: x: 4, y: 4, z: 4, core: 2. Of those that a mesh axis runs over, the one named last changes fastest.
Arguments:
- query_first: bfloat16 [8, 2048, 1024], P('dp', 'sp'), may hold values from -200 to 200
- key_first: bfloat16 [8, 2048, 1024], P('dp', 'sp'), may hold values from -8 to 8
- query_second: bfloat16 [8, 2048, 1024], P('dp', 'sp'), may hold values from -200 to 200
- key_second: bfloat16 [8, 2048, 1024], P('dp', 'sp'), may hold values from -8 to 8
- value_rows: bfloat16 [8, 2048, 2048], P('dp', 'sp'), may hold values from -6 to 6
- mix_lambda: float32 [16], replicated, may hold values from 0.3 to 0.8
- head_gain: float32 [128], replicated, may hold values from 0.1 to 1.9
- residual: bfloat16 [8, 2048, 2048], P('dp', 'sp'), may hold values from -6 to 6
- out_weight: bfloat16 [2048, 2048], replicated, may hold values from -0.125 to 0.125
- norm_gain: float32 [2048], replicated, may hold values from 0.1 to 1.9
- routes: int32 [8, 2048, 4], P('dp', 'sp'), may hold values from 0 to 127, all different within a row; in each aligned block of 128 rows (0 to 127, 128 to 255, ..., all dimensions but the last counted through in order) at most 6 rows name the same one
- route_weights: float32 [8, 2048, 4], P('dp', 'sp'), may hold values from 0.1 to 1
- gate_weight: bfloat16 [128, 2048, 1024], P(('sp', 'dp')), may hold values from -0.375 to 0.375
- up_weight: bfloat16 [128, 2048, 1024], P(('sp', 'dp')), may hold values from -0.375 to 0.375
- down_weight: bfloat16 [128, 1024, 2048], P(('sp', 'dp')), may hold values from -0.046875 to 0.046875
Outputs:
- layer_out: bfloat16 [8, 2048, 2048], P('dp', 'sp')
Inputs may be any that keep to these rules, and one draw needn't show every extreme that they name: `routes`: within the rows of one device (aligned blocks of 128 positions of a sequence) no expert is named more than 6 times, a bound that some block reaches.
All inputs are finite; a program needn't handle non-finite values.
Results may differ from a plain program's by a relative error of at most 0.0075.
Values may be sent and summed in bfloat16 or wider, within the bound.
A program may use at most 128 MiB of HBM per device.

v0:
```python
import jax
import jax.numpy as jnp
from jax import lax
from jax.experimental import pallas as pl
from jax.experimental.pallas import tpu as pltpu
from jax.sharding import PartitionSpec as P

MESH = pl.DeviceIdType.MESH
RING = 4
CAP = 6
OFFSETS = (
    (0, 1), (1, 0), (0, 3), (3, 0), (1, 1), (3, 3), (1, 3), (3, 1),
    (0, 2), (2, 0), (1, 2), (2, 1), (3, 2), (2, 3), (2, 2),
)
EDGE = 128
WIDE = 256
ENDS = 2


def layer_kernel(
    q1_hbm, k1_hbm, q2_hbm, k2_hbm, v_hbm, lambda_hbm, hgain_hbm,
    res_hbm, wo_hbm, gain_hbm, routes_hbm, rweights_hbm, wg_hbm, wu_hbm, wd_hbm,
    out_hbm,
    q1, k1, q2, k2, vals, lamv, hgain, res, gain, routes, rweights,
    packed, keys, valt, mix, hsend, heads_in,
    wg, wu, wd, mixed, gath, slab, xin, acc, hid, back, rin,
    part_out, part_in, sum_out, sum_in, own, pick, wsel, meta, done_out,
    lsem, as_, ar, hs, hr, osem,
    wsem, meta_s, meta_r, xs, xr, cs, cr, ds, dr, bs, br, ps, pr, ts, tr,
):
    f32, bf16 = jnp.float32, jnp.bfloat16
    sp, dp = lax.axis_index("sp"), lax.axis_index("dp")
    z, y = sp // RING, sp % RING
    x, c = dp // 2, dp % 2
    partner = x * 2 + (1 - c)
    rows, width = res.shape
    nsp, slots = slab.shape[0], slab.shape[1]
    ndp = gath.shape[0]
    filled = nsp * slots
    half = wg.shape[1]
    hd = q1.shape[1] // nsp
    hv = vals.shape[1] // nsp
    wide = (width - 2 * ENDS * EDGE) // WIDE
    n = wide + 2 * ENDS

    def head_chunk(k):
        return (k, pl.multiple_of(k * EDGE, EDGE), EDGE)

    def middle(k):
        return (k, pl.multiple_of(ENDS * EDGE + (k - ENDS) * WIDE, EDGE), WIDE)

    def tail_chunk(k):
        return (k, pl.multiple_of(width - (n - k) * EDGE, EDGE), EDGE)

    def loop(begin, end, step):
        def body(k, carry):
            step(k)
            return carry

        lax.fori_loop(begin, end, body, 0)

    def cols(chunk):
        return pl.ds(chunk[1], chunk[2])

    def peer(i, sign=1):
        dz, dy = OFFSETS[i]
        return ((z + sign * dz + RING) % RING) * RING + (y + sign * dy + RING) % RING

    def xpeer(i, sign=1):
        return (x + sign * (i + 1) + RING) % RING

    def remote(src, dst, ssem, rsem, to):
        return pltpu.make_async_remote_copy(
            src_ref=src, dst_ref=dst, send_sem=ssem, recv_sem=rsem,
            device_id=to, device_id_type=MESH,
        )

    barrier = pltpu.get_barrier_semaphore()
    for i in range(nsp - 1):
        pl.semaphore_signal(barrier, inc=1, device_id=(peer(i), dp), device_id_type=MESH)
    for i in range(1, ndp):
        pl.semaphore_signal(barrier, inc=1, device_id=(sp, (dp + i) % ndp), device_id_type=MESH)

    loads = [
        pltpu.make_async_copy(src, dst, lsem.at[i])
        for i, (src, dst) in enumerate(
            (
                (q1_hbm, q1), (q2_hbm, q2), (k1_hbm, k1), (k2_hbm, k2),
                (routes_hbm, routes), (rweights_hbm, rweights), (v_hbm, vals),
                (lambda_hbm, lamv), (hgain_hbm, hgain), (gain_hbm, gain), (res_hbm, res),
            )
        )
    ]
    for load in loads:
        load.start()
    wo_a = pltpu.make_async_copy(wo_hbm.at[:, pl.ds(0, half)], wg, wsem.at[0])
    wo_b = pltpu.make_async_copy(wo_hbm.at[:, pl.ds(half, half)], wu, wsem.at[1])
    wd_c = pltpu.make_async_copy(wd_hbm, wd, wsem.at[2])
    wg_c = pltpu.make_async_copy(wg_hbm, wg, wsem.at[3])
    wu_c = pltpu.make_async_copy(wu_hbm, wu, wsem.at[4])

    for step, (base, one, two) in enumerate(((0, q1, q2), (2 * hd, k1, k2))):
        loads[2 * step].wait()
        loads[2 * step + 1].wait()
        for g in range(nsp // 2):
            pair = slice(g * 2 * hd, (g + 1) * 2 * hd)
            a, b = one[:, pair], two[:, pair]
            at = slice(base, base + 2 * hd)
            packed[2 * g, :, at] = jnp.concatenate([a[:, :hd], b[:, :hd]], axis=1)
            packed[2 * g + 1, :, at] = jnp.concatenate([a[:, hd:], b[:, hd:]], axis=1)
    loads[4].wait()
    loads[5].wait()
    meta[dp, :RING] = routes[...].astype(f32)
    meta[dp, RING:] = rweights[...]

    pl.semaphore_wait(barrier, nsp - 1 + ndp - 1)

    def qkv(dst, src, which):
        at = pl.ds(0, 4 * hd) if which == 0 else pl.ds(4 * hd, hv)
        return remote(
            packed.at[dst, :, at], keys.at[src, :, at], as_.at[which, dst], ar.at[which, src],
            (dst, dp),
        )

    def meta_copy(i, src):
        return remote(
            meta.at[src], meta.at[src], meta_s.at[i], meta_r.at[i], (sp, (dp + i) % ndp)
        )

    for i in range(nsp - 1):
        qkv(peer(i), sp, 0).start()
    for i in range(1, ndp):
        meta_copy(i, dp).start()
    loads[6].wait()
    for h in range(nsp):
        packed[h, :, 4 * hd :] = vals[:, h * hv : (h + 1) * hv]
    keys[sp] = packed[sp]
    wo_a.start()
    wo_b.start()
    wd_c.start()
    for load in loads[7:]:
        load.wait()

    for i in range(1, ndp):
        meta_copy(i, (dp - i + ndp) % ndp).wait_recv()
    before = (
        lax.broadcasted_iota(jnp.int32, (rows, rows), 0)
        < lax.broadcasted_iota(jnp.int32, (rows, rows), 1)
    ).astype(bf16)
    expert = (lax.broadcasted_iota(jnp.int32, (nsp, rows), 0) * ndp + dp).astype(f32)
    place = lax.broadcasted_iota(jnp.int32, (nsp, slots, rows), 1).astype(f32)

    def table(b, carry):
        info = meta[b]
        named = jnp.zeros((nsp, rows), f32)
        weight = jnp.zeros((nsp, rows), f32)
        for t in range(RING):
            hit = (info[t : t + 1, :] == expert).astype(f32)
            named = named + hit
            weight = weight + hit * info[t + RING : t + RING + 1, :]
        rank = jnp.dot(named.astype(bf16), before, preferred_element_type=f32)
        slot = jnp.where(named > 0.0, rank + (b * CAP).astype(f32), -1.0)
        match = (slot[:, None, :] == place).astype(f32)
        at = pl.ds(pl.multiple_of(b * rows, rows), rows)
        pick[:, at] = match.reshape(filled, rows).astype(bf16)
        scaled = (match * weight[:, None, :]).reshape(filled, rows)
        wsel[(b % 2) * RING + b // 2] = jnp.transpose(scaled).astype(bf16)
        return carry

    lax.fori_loop(0, ndp, table, 0)

    for i in range(nsp - 1):
        qkv(peer(i), sp, 0).wait_send()
    for i in range(nsp - 1):
        qkv(peer(i), sp, 1).start()

    block = 2 * rows
    blocks = nsp // 2
    lane_of = lax.broadcasted_iota(jnp.int32, (1, nsp), 1)
    lam = jnp.sum(jnp.where(lane_of == sp, lamv[...], 0.0), axis=1, keepdims=True)
    scale = hd ** (-0.5) * 1.4426950408889634

    def heads(dst, src):
        at = pl.ds(pl.multiple_of(src * hv, hv), hv)
        return remote(hsend.at[dst], heads_in.at[:, at], hs.at[dst], hr.at[src], (dst, dp))

    def folded(value, op):
        return op(value.reshape(-1, 8, value.shape[1]), axis=0)

    def arrived(i, which):
        for src in (2 * i, 2 * i + 1):

            @pl.when(src != sp)
            def _():
                qkv(src, src, which).wait_recv()

    below = lax.broadcasted_iota(jnp.int32, (block, 2 * block), 0)
    across = lax.broadcasted_iota(jnp.int32, (block, 2 * block), 1)
    seen = below <= jnp.where(across < block, across, across - block)
    lane = lax.broadcasted_iota(jnp.int32, (block, 2 * hd), 1)

    def base(i):
        return 0 if i % 2 == 0 else (blocks - 1) * block

    def tile_of(i, j):
        return slice(base(i) + j * block, base(i) + (j + 1) * block)

    def score(i):
        arrived(i, 0)
        query = keys[2 * i : 2 * i + 2, :, : 2 * hd].reshape(block, 2 * hd)
        zero = jnp.zeros_like(query)
        both = jnp.concatenate(
            [jnp.where(lane < hd, query, zero), jnp.where(lane < hd, zero, query)], axis=0
        )
        top = jnp.full((8, 2 * block), -1e30, f32)
        for j in range(i + 1):
            key = keys[2 * j : 2 * j + 2, :, 2 * hd : 4 * hd].reshape(block, 2 * hd)
            value = lax.dot_general(
                key, both, (((1,), (1,)), ((), ())), preferred_element_type=f32
            )
            if j == i:
                value = jnp.where(seen, value, -1e30)
            acc[tile_of(i, j), :] = value
            top = jnp.maximum(top, folded(value, jnp.max))
        return jnp.max(top, axis=0, keepdims=True)

    def normalize(i, top):
        total = jnp.zeros((8, 2 * block), f32)
        for j in range(i + 1):
            value = jnp.exp2((acc[tile_of(i, j), :] - top) * scale)
            acc[tile_of(i, j), :] = value
            total = total + folded(value, jnp.sum)
        total = jnp.sum(total, axis=0, keepdims=True)
        share = 1.0 / total[:, :block]
        taken = lam / total[:, block:]
        for j in range(i + 1):
            at = tile_of(i, j)
            value = acc[at, :block] * share - acc[at, block:] * taken
            mix[i * (i + 1) // 2 + j] = value.astype(bf16)

    def weigh(i):
        arrived(i, 1)
        turned = jnp.transpose(keys[2 * i : 2 * i + 2, :, 4 * hd :].reshape(block, hv).astype(f32))
        valt[:, i * block : (i + 1) * block] = turned.astype(bf16)
        begin = i * (i + 1) // 2
        tiles = mix[begin : begin + i + 1].reshape((i + 1) * block, block)
        return jnp.dot(valt[:, : (i + 1) * block], tiles, preferred_element_type=f32)

    def settle(i, raw):
        size = lax.rsqrt(jnp.mean(raw * raw, axis=0, keepdims=True) + 1e-06)
        done = (jnp.transpose(raw * size) * hgain[...]).astype(bf16)
        hsend[2 * i : 2 * i + 2] = done.reshape(2, rows, hv)
        for dst in (2 * i, 2 * i + 1):

            @pl.when(dst != sp)
            def _():
                heads(dst, sp).start()

            @pl.when(dst == sp)
            def _():
                heads_in[:, pl.ds(pl.multiple_of(sp * hv, hv), hv)] = hsend[dst]

    def settle_all(which):
        raw = weigh(which[0])
        for n_th, i in enumerate(which):
            following = weigh(which[n_th + 1]) if n_th + 1 < len(which) else None
            settle(i, raw)
            raw = following

    done_to = 0
    top = score(0)
    for i in range(blocks):
        next_top = score(i + 1) if i + 1 < blocks else None
        normalize(i, top)
        top = next_top
        ready = {blocks - 3: i - 1, blocks - 2: i, blocks - 1: i + 1}.get(i, 0)
        if ready > done_to:
            settle_all(range(done_to, ready))
            done_to = ready

    mixed[...] = res[...].astype(f32)
    wo_a.wait()
    wo_b.wait()

    def project(g, carry):
        pair = (g // RING) * RING + (g % RING + 2 * (1 - g // RING)) % RING
        for s in range(2):
            src = 2 * pair + s

            @pl.when(src != sp)
            def _():
                heads(src, src).wait_recv()

        deep = pl.ds(pl.multiple_of(pair * 2 * hv, 2 * hv), 2 * hv)
        part = heads_in[:, deep]
        mixed[:, :half] += jnp.dot(part, wg[deep, :], preferred_element_type=f32)
        mixed[:, half:] += jnp.dot(part, wu[deep, :], preferred_element_type=f32)
        return carry

    lax.fori_loop(0, nsp // 2, project, 0)
    wg_c.start()
    wu_c.start()
    square = jnp.zeros((rows, 128), f32)
    for t in range(width // 128):
        value = mixed[:, t * 128 : (t + 1) * 128]
        square = square + value * value
    factor = lax.rsqrt(jnp.sum(square, axis=1, keepdims=True) / width + 1e-06)

    def gx(chunk, i, src):
        k = chunk[0]
        return remote(
            gath.at[dp, :, cols(chunk)], gath.at[src * 2 + c, :, cols(chunk)], xs.at[k, i], xr.at[k, i],
            (sp, xpeer(i) * 2 + c),
        )

    def gown(chunk, src):
        k = chunk[0]
        return remote(
            gath.at[dp, :, cols(chunk)], gath.at[src, :, cols(chunk)], cs.at[k, 3], cr.at[k, 3],
            (sp, partner),
        )

    def gfwd(chunk, i, core):
        k = chunk[0]
        at = xpeer(i, -1) * 2 + core
        return remote(
            gath.at[at, :, cols(chunk)], gath.at[at, :, cols(chunk)], cs.at[k, i], cr.at[k, i],
            (sp, partner),
        )

    def gsend(chunk):
        for i in (1, 0, 2):
            gx(chunk, i, x).start()
        gown(chunk, dp).start()

    widths = [EDGE] * ENDS + [WIDE] * wide + [EDGE] * ENDS
    static = [(k, sum(widths[:k]), w) for k, w in enumerate(widths)]
    for k, chunk in enumerate(static):
        at = slice(chunk[1], chunk[1] + chunk[2])
        gath[dp, :, at] = (mixed[:, at] * factor * gain[:, at]).astype(bf16)
        if k > 0:
            gsend(static[k - 1])
    gsend(static[-1])
    acc[...] = jnp.zeros_like(acc)

    def exchange(out_buf, in_buf, ssem, rsem, chunk, i, src, dst):
        k = chunk[0]
        return remote(
            out_buf.at[dst, :, cols(chunk)], in_buf.at[src, :, cols(chunk)],
            ssem.at[k, i], rsem.at[k, i], (dst, dp),
        )

    def send_all(out_buf, in_buf, ssem, rsem, chunk):
        for i in range(nsp - 1):
            exchange(out_buf, in_buf, ssem, rsem, chunk, i, sp, peer(i)).start()

    def wait_all(out_buf, in_buf, ssem, rsem, chunk):
        for i in range(nsp - 1):
            exchange(out_buf, in_buf, ssem, rsem, chunk, i, peer(i, -1), peer(i)).wait_recv()

    def dispatch(chunk):
        for i in (0, 2, 1):
            gx(chunk, i, xpeer(i, -1)).wait_recv()
            gfwd(chunk, i, c).start()
        gown(chunk, partner).wait_recv()
        for i in (0, 2, 1):
            gfwd(chunk, i, 1 - c).wait_recv()
        tokens = gath[:, :, cols(chunk)].reshape(ndp * rows, chunk[2])
        group = nsp // 4

        def build(g, carry):
            sel = pick[pl.ds(pl.multiple_of(g * group * slots, group * slots), group * slots), :]
            made = jnp.dot(sel, tokens, preferred_element_type=f32).astype(bf16)
            slab[pl.ds(g * group, group), :, cols(chunk)] = made.reshape(group, slots, chunk[2])
            return carry

        lax.fori_loop(0, 4, build, 0)
        xin[sp, :, cols(chunk)] = slab[sp, :, cols(chunk)]
        send_all(slab, xin, ds, dr, chunk)

    def each(action, end=n):
        loop(0, ENDS, lambda k: action(head_chunk(k)))
        loop(ENDS, ENDS + wide, lambda k: action(middle(k)))
        loop(ENDS + wide, end, lambda k: action(tail_chunk(k)))

    each(dispatch)
    wg_c.wait()
    wu_c.wait()
    tile = 256
    span = acc.shape[1]
    per = span // tile

    def receive(chunk):
        wait_all(slab, xin, ds, dr, chunk)

        def units(t, carry):
            at = pl.ds(pl.multiple_of(t * tile, tile), tile)
            to = pl.ds(pl.multiple_of((t % per) * tile, tile), tile)
            low = pl.ds(pl.multiple_of((t // per) * filled, filled), filled)
            high = pl.ds(pl.multiple_of((t // per + half // span) * filled, filled), filled)
            taken = xin[:, :, cols(chunk)].reshape(filled, chunk[2])
            gate = jnp.dot(taken, wg[cols(chunk), at], preferred_element_type=f32)
            upper = jnp.dot(taken, wu[cols(chunk), at], preferred_element_type=f32)
            acc[low, to] += gate
            acc[high, to] += upper
            return carry

        lax.fori_loop(0, half // tile, units, 0)

    each(receive, n - 1)

    wait_all(slab, xin, ds, dr, static[-1])

    def gated(t, carry):
        at = pl.ds(pl.multiple_of(t * tile, tile), tile)
        to = pl.ds(pl.multiple_of((t % per) * tile, tile), tile)
        low = pl.ds(pl.multiple_of((t // per) * filled, filled), filled)
        high = pl.ds(pl.multiple_of((t // per + half // span) * filled, filled), filled)
        taken = xin[:, :, cols(static[-1])].reshape(filled, EDGE)
        deep = cols(static[-1])
        gate = acc[low, to] + jnp.dot(taken, wg[deep, at], preferred_element_type=f32)
        upper = acc[high, to] + jnp.dot(taken, wu[deep, at], preferred_element_type=f32)
        gate = jnp.minimum(gate, 7.0)
        upper = jnp.clip(upper, -7.0, 7.0) + 1.0
        hid[:, at] = (upper * gate / (1.0 + jnp.exp(-1.702 * gate))).astype(bf16)
        return carry

    lax.fori_loop(0, half // tile, gated, 0)
    wd_c.wait()

    def down(chunk):
        made = jnp.dot(hid[...], wd[:, cols(chunk)], preferred_element_type=f32).astype(bf16)
        back[:, :, cols(chunk)] = made.reshape(nsp, slots, chunk[2])
        rin[sp, :, cols(chunk)] = back[sp, :, cols(chunk)]
        send_all(back, rin, bs, br, chunk)

    each(down)

    def part_copy(chunk):
        k = chunk[0]
        return remote(
            part_out.at[:, :, cols(chunk)], part_in.at[:, :, cols(chunk)], ps.at[k], pr.at[k],
            (sp, partner),
        )

    def total_copy(chunk, i, src):
        k = chunk[0]
        return remote(
            sum_out.at[xpeer(i), :, cols(chunk)], sum_in.at[src, :, cols(chunk)],
            ts.at[k, i], tr.at[k, i], (sp, xpeer(i) * 2 + c),
        )

    def weighted(core, chunk):
        sel = wsel[pl.ds(core * RING, RING)].reshape(RING * rows, filled)
        taken = rin[:, :, cols(chunk)].reshape(filled, chunk[2])
        made = jnp.dot(sel, taken, preferred_element_type=f32)
        return made.reshape(RING, rows, chunk[2])

    def out_copy(chunk):
        return pltpu.make_async_copy(
            done_out.at[:, cols(chunk)], out_hbm.at[:, cols(chunk)], osem.at[chunk[0]]
        )

    def combine(chunk):
        wait_all(back, rin, bs, br, chunk)
        part_out[:, :, cols(chunk)] = weighted(1 - c, chunk).astype(bf16)
        part_copy(chunk).start()
        own[chunk[0] % 2, :, :, : chunk[2]] = weighted(c, chunk)

    def add_parts(chunk):
        part_copy(chunk).wait_recv()
        mine = own.at[chunk[0] % 2]
        for i in (1, 0, 2):
            to = xpeer(i)
            sums = mine[to, :, : chunk[2]] + part_in[to, :, cols(chunk)].astype(f32)
            sum_out[to, :, cols(chunk)] = sums.astype(bf16)
        mixed[:, cols(chunk)] += mine[x, :, : chunk[2]] + part_in[x, :, cols(chunk)].astype(f32)
        for i in (1, 0, 2):
            total_copy(chunk, i, x).start()

    def finish(chunk):
        value = mixed[:, cols(chunk)]
        for i in range(3):
            total_copy(chunk, i, xpeer(i, -1)).wait_recv()
            value = value + sum_in[xpeer(i, -1), :, cols(chunk)].astype(f32)
        done_out[:, cols(chunk)] = value.astype(bf16)
        out_copy(chunk).start()

    def step(chunk, earlier=None):
        combine(chunk)
        if earlier is not None:
            finish(earlier)
        add_parts(chunk)

    begin, end = ENDS, ENDS + wide
    loop(0, begin, lambda k: step(head_chunk(k)))
    loop(begin, 2 * begin, lambda k: step(middle(k), head_chunk(k - ENDS)))
    loop(2 * begin, end, lambda k: step(middle(k), middle(k - ENDS)))
    loop(end, n, lambda k: step(tail_chunk(k)))
    loop(end - ENDS, end, lambda k: finish(middle(k)))
    loop(end, n, lambda k: finish(tail_chunk(k)))

    for i in range(nsp - 1):
        qkv(peer(i), sp, 1).wait_send()
        heads(peer(i), sp).wait_send()
    for i in range(1, ndp):
        meta_copy(i, dp).wait_send()

    def drain(chunk):
        for i in range(3):
            gx(chunk, i, x).wait_send()
            gfwd(chunk, i, c).wait_send()
            total_copy(chunk, i, x).wait_send()
        gown(chunk, dp).wait_send()
        part_copy(chunk).wait_send()
        for i in range(nsp - 1):
            exchange(slab, xin, ds, dr, chunk, i, sp, peer(i)).wait_send()
            exchange(back, rin, bs, br, chunk, i, sp, peer(i)).wait_send()
        out_copy(chunk).wait()

    each(drain)


def on_device(
    query_first,
    key_first,
    query_second,
    key_second,
    value_rows,
    mix_lambda,
    head_gain,
    residual,
    out_weight,
    norm_gain,
    routes,
    route_weights,
    gate_weight,
    up_weight,
    down_weight,
):
    nsp, ndp = lax.axis_size("sp"), lax.axis_size("dp")
    rows, width = residual.shape[1:]
    hidden = gate_weight.shape[2]
    qk = query_first.shape[2]
    hv = head_gain.shape[0]
    packed = 4 * qk // nsp + hv
    slots = CAP * ndp
    filled = slots * nsp
    n = (width - 2 * ENDS * EDGE) // WIDE + 2 * ENDS
    bf16, f32 = jnp.bfloat16, jnp.float32
    hbm = pl.BlockSpec(memory_space=pl.ANY)
    vmem = pltpu.VMEM
    dma = pltpu.SemaphoreType.DMA
    out = pl.pallas_call(
        layer_kernel,
        out_shape=jax.ShapeDtypeStruct((rows, width), bf16),
        in_specs=[hbm] * 15,
        out_specs=hbm,
        scratch_shapes=[
            vmem((rows, qk), bf16), vmem((rows, qk), bf16),
            vmem((rows, qk), bf16), vmem((rows, qk), bf16),
            vmem((rows, nsp * hv), bf16),
            vmem((1, nsp), f32), vmem((1, hv), f32), vmem((rows, width), bf16),
            vmem((1, width), f32), vmem((RING, rows), jnp.int32), vmem((RING, rows), f32),
            vmem((nsp, rows, packed), bf16),
            vmem((nsp, rows, packed), bf16),
            vmem((hv, nsp * rows), bf16),
            vmem((nsp * (nsp + 2) // 8, 2 * rows, 2 * rows), bf16),
            vmem((nsp, rows, hv), bf16),
            vmem((rows, nsp * hv), bf16),
            vmem((width, hidden), bf16), vmem((width, hidden), bf16),
            vmem((hidden, width), bf16),
            vmem((rows, width), f32),
            vmem((ndp, rows, width), bf16),
            vmem((nsp, slots, width), bf16), vmem((nsp, slots, width), bf16),
            vmem((max(4 * filled, (nsp - 1) * 2 * rows), hidden // 2), f32), vmem((filled, hidden), bf16),
            vmem((nsp, slots, width), bf16), vmem((nsp, slots, width), bf16),
            vmem((RING, rows, width), bf16), vmem((RING, rows, width), bf16),
            vmem((RING, rows, width), bf16), vmem((RING, rows, width), bf16),
            vmem((2, RING, rows, WIDE), f32),
            vmem((filled, ndp * rows), bf16),
            vmem((ndp, rows, filled), bf16),
            vmem((ndp, 8, rows), f32),
            vmem((rows, width), bf16),
            dma((11,)), dma((2, nsp)), dma((2, nsp)), dma((nsp,)), dma((nsp,)), dma((n,)),
            dma((5,)), dma((ndp,)), dma((ndp,)),
            dma((n, 3)), dma((n, 3)), dma((n, 4)), dma((n, 4)),
            dma((n, nsp)), dma((n, nsp)), dma((n, nsp)), dma((n, nsp)),
            dma((n,)), dma((n,)), dma((n, 3)), dma((n, 3)),
        ],
        compiler_params=pltpu.CompilerParams(
            collective_id=1, has_side_effects=True, vmem_limit_bytes=67000000
        ),
        name="layer",
    )(
        query_first[0], key_first[0], query_second[0], key_second[0], value_rows[0],
        mix_lambda[None, :], head_gain[None, :], residual[0], out_weight, norm_gain[None, :],
        routes[0].T, route_weights[0].T, gate_weight[0], up_weight[0], down_weight[0],
    )
    return out[None]


def solution(mesh):
    return jax.shard_map(
        on_device,
        mesh=mesh,
        in_specs=(
            P("dp", "sp", None),
            P("dp", "sp", None),
            P("dp", "sp", None),
            P("dp", "sp", None),
            P("dp", "sp", None),
            P(),
            P(),
            P("dp", "sp", None),
            P(),
            P(),
            P("dp", "sp", None),
            P("dp", "sp", None),
            P(("sp", "dp"), None, None),
            P(("sp", "dp"), None, None),
            P(("sp", "dp"), None, None),
        ),
        out_specs=P("dp", "sp", None),
        check_vma=False,
    )
```

profile of v0, /device:TPU:9, one launch (start us, length us, event | category | flops | bytes accessed | tf_op | source)
XLA Modules:
  0.0 141.4 jit_solution(12636163811460919435)
XLA Ops:
  0.0 139.5 %layer.1 = bf16[128,2048]{1,0:T(8,128)(2,1)} custom-call(bf16[128,1024]{1,0:T(8,128)(2,1)} %bitcast.25, bf16[128,1024]{1,0:T(8,128)(2,1)} %bitcast.26, bf16[128,1024]{1,0:T(8,128)(2,1)} %bitcast.27, bf16[128,1024]{1,0:T(8,128)(2,1)} %bitcast.28, bf16[128,2048]{1,0:T(8,128)(2,1)} %bitcast.23, f32[1,16]{1,0:T(1,128)} %bitcast.32, f32[1,128]{1,0:T(1,128)} %bitcast.33, ...), custom_call_target="tpu_custom_call" | custom-call | tf_op jit(solution)/shard_map/layer/pallas_call | solution.py:554
  139.6 1.9 %copy.17 = bf16[1,128,2048]{2,1,0:T(8,128)(2,1)} copy(bf16[1,128,2048]{2,1,0:T(8,128)(2,1)} %bitcast.22) | data formatting | bytes 1048576
where the time goes:
time: 143 us; the launch traced here: 141 us
  Pallas kernels  140 us (98%)
  local copies, waits for them, and re-layouts  1.88 us (1%)
    pallas_call x1, Pallas kernels, on_device(): pl.pallas_call(layer_kernel, out_shape=jax.ShapeDtypeStruct((rows, width)...  140 us

commit v1 on v0

--- a/solution.py
+++ b/solution.py
@@ -498,7 +498,6 @@
     loop(2 * begin, end, lambda k: step(middle(k), middle(k - ENDS)))
     loop(end, n, lambda k: step(tail_chunk(k)))
     loop(end - ENDS, end, lambda k: finish(middle(k)))
-    loop(end, n, lambda k: finish(tail_chunk(k)))
 
     for i in range(nsp - 1):
         qkv(peer(i), sp, 1).wait_send()
@@ -506,19 +505,25 @@
     for i in range(1, ndp):
         meta_copy(i, dp).wait_send()
 
-    def drain(chunk):
+    def left(chunk):
         for i in range(3):
             gx(chunk, i, x).wait_send()
             gfwd(chunk, i, c).wait_send()
-            total_copy(chunk, i, x).wait_send()
         gown(chunk, dp).wait_send()
         part_copy(chunk).wait_send()
         for i in range(nsp - 1):
             exchange(slab, xin, ds, dr, chunk, i, sp, peer(i)).wait_send()
             exchange(back, rin, bs, br, chunk, i, sp, peer(i)).wait_send()
+
+    def left_last(chunk):
+        for i in range(3):
+            total_copy(chunk, i, x).wait_send()
         out_copy(chunk).wait()
 
-    each(drain)
+    each(left)
+    each(left_last, end)
+    loop(end, n, lambda k: finish(tail_chunk(k)))
+    loop(end, n, lambda k: left_last(tail_chunk(k)))
 
 
 def on_device(

time: 143 us -> 143 us (level)
  no operation moved by 1% of the time
where the time goes in v1:
time: 143 us; the launch traced here: 141 us
  Pallas kernels  139 us (97%)
  local copies, waits for them, and re-layouts  1.88 us (1%)
    pallas_call x1, Pallas kernels, on_device(): pl.pallas_call(layer_kernel, out_shape=jax.ShapeDtypeStruct((rows, width)...  139 us

profile of v1, /device:TPU:9, one launch (start us, length us, event | category | flops | bytes accessed | tf_op | source)
XLA Modules:
  0.0 141.3 jit_solution(10859496128787717379)
XLA Ops:
  0.0 139.4 %layer.1 = bf16[128,2048]{1,0:T(8,128)(2,1)} custom-call(bf16[128,1024]{1,0:T(8,128)(2,1)} %bitcast.25, bf16[128,1024]{1,0:T(8,128)(2,1)} %bitcast.26, bf16[128,1024]{1,0:T(8,128)(2,1)} %bitcast.27, bf16[128,1024]{1,0:T(8,128)(2,1)} %bitcast.28, bf16[128,2048]{1,0:T(8,128)(2,1)} %bitcast.23, f32[1,16]{1,0:T(1,128)} %bitcast.32, f32[1,128]{1,0:T(1,128)} %bitcast.33, ...), custom_call_target="tpu_custom_call" | custom-call | tf_op jit(solution)/shard_map/layer/pallas_call | solution.py:559
  139.4 1.9 %copy.17 = bf16[1,128,2048]{2,1,0:T(8,128)(2,1)} copy(bf16[1,128,2048]{2,1,0:T(8,128)(2,1)} %bitcast.22) | data formatting | bytes 1048576
